TPU v7x, 32 devices: a whole 2x2x4 slice. The times are simulated.
32 devices in a mesh: ep: 8 (over z, y), tp: 4 (over x, core).
Axes of the slice: x: 2, y: 2, z: 4, core: 2. Of those that a mesh axis runs over, the one named last changes fastest.
Arguments:
- queries: bfloat16 [1024, 512], P('ep', 'tp'), may hold values from -8 to 8
- key_cache: bfloat16 [4, 64, 1024], P('tp', None, 'ep'), may hold values from -4.5 to 4.5
- value_cache: bfloat16 [4, 64, 1024], P('tp', None, 'ep'), may hold values from -6 to 6
- cum_gate: float32 [4, 1024], P('tp'), may hold values from -256 to 0, as said below
- out_weight: bfloat16 [512, 2048], replicated, may hold values from -1 to 1
- routed_input: bfloat16 [2048, 2048], P('ep'), may hold values from -6 to 6
- norm_gain: bfloat16 [2048], replicated, may hold values from 0.099609375 to 1.8984375
- routes: int32 [2048, 2], P('ep'), may hold values from 0 to 7, all different within a row; in each aligned block of 64 rows (0 to 63, 64 to 127, ...) at most 24 rows name the same one
- route_weight: float32 [2048, 2], P('ep'), may hold values from 0.2 to 1
- expert_gate: bfloat16 [8, 2048, 1024], P('ep', None, 'tp'), may hold values from -0.125 to 0.125
- expert_up: bfloat16 [8, 2048, 1024], P('ep', None, 'tp'), may hold values from -0.125 to 0.125
- expert_down: bfloat16 [8, 1024, 2048], P('ep', 'tp'), may hold values from -0.1875 to 0.1875
Outputs:
- mixed_out: bfloat16 [1024, 2048], P(('ep', 'tp'))
- expert_out: bfloat16 [2048, 2048], P(('ep', 'tp'))
Inputs may be any that keep to these rules, and one draw needn't show every extreme that they name: `cum_gate`: Non-increasing along positions in every head. `routes`: each row names 2 different experts. In each aligned block of 64 rows (the rows of one device) no expert is named by more than 24 rows, a bound that some block reaches.
All inputs are finite; a program needn't handle non-finite values.
Results may differ from a plain program's by a relative error of at most 0.012.
Values may be sent and summed in bfloat16 or wider, within the bound.
A program may use at most 64 MiB of HBM per device.

v0:
```python
import jax
import jax.numpy as jnp
from jax import lax
from jax.sharding import PartitionSpec as P


def slot_chooser(route_rows, expert_count, capacity):
    token_rows, top_count = route_rows.shape
    flat = route_rows.reshape(token_rows * top_count)
    same = (flat[:, None] == jnp.arange(expert_count, dtype=jnp.int32)[None, :]).astype(jnp.int32)
    earlier = jnp.cumsum(same, axis=0) - same
    rank = jnp.sum(earlier * same, axis=1)
    slot = flat * capacity + rank
    chosen = slot[:, None] == jnp.arange(expert_count * capacity, dtype=jnp.int32)[None, :]
    return chosen.astype(jnp.bfloat16).reshape(token_rows, top_count, expert_count * capacity)


def rms_rows(source, norm_gain):
    widened = source.astype(jnp.float32)
    scale = lax.rsqrt(jnp.mean(widened * widened, axis=-1, keepdims=True) + 1e-06)
    return (widened * scale * norm_gain.astype(jnp.float32)).astype(jnp.bfloat16)


def mixer_half(queries, key_cache, value_cache, cum_gate, out_weight):
    seq_rows = queries.shape[0]
    local_heads = key_cache.shape[0]
    head_size = key_cache.shape[1]
    group = queries.shape[1] // (local_heads * head_size)
    own_start = lax.axis_index("ep") * seq_rows
    query_heads = queries.reshape(seq_rows, local_heads, group, head_size)
    query_pos = own_start + jnp.arange(seq_rows, dtype=jnp.int32)
    gate_query = lax.dynamic_slice_in_dim(cum_gate, own_start, seq_rows, 1)
    gate_rows = jnp.transpose(gate_query)[:, :, None, None]
    scale = head_size ** (-0.5)
    best_start = jnp.full((seq_rows, local_heads, group), -jnp.inf, jnp.float32)
    total_start = jnp.zeros((seq_rows, local_heads, group), jnp.float32)
    summed_start = jnp.zeros((seq_rows, local_heads * group * head_size), jnp.float32)
    pieces = (
        lax.all_gather(key_cache, "ep", axis=2, tiled=True),
        lax.all_gather(value_cache, "ep", axis=2, tiled=True),
    )

    def update(state):
        best, total, summed = state
        key_piece, value_piece = pieces
        width = key_piece.shape[2]
        scores = (
            jnp.einsum("thgd,hds->thgs", query_heads, key_piece, preferred_element_type=jnp.float32)
            * scale
        )
        scores = scores + gate_rows - cum_gate[None, :, None, :]
        key_pos = jnp.arange(width, dtype=jnp.int32)
        allowed = key_pos[None, :] <= query_pos[:, None]
        scores = jnp.where(allowed[:, None, None, :], scores, -jnp.inf)
        new_best = jnp.max(scores, axis=-1)
        factor = jnp.exp(best - new_best)
        weights = jnp.exp(scores - new_best[..., None])
        new_total = total * factor + jnp.sum(weights, axis=-1)
        product = jnp.einsum(
            "thgs,hds->thgd",
            weights.astype(jnp.bfloat16),
            value_piece,
            preferred_element_type=jnp.float32,
        )
        new_summed = summed.reshape(product.shape) * factor[..., None] + product
        return (new_best, new_total, new_summed.reshape(seq_rows, local_heads * group * head_size))

    best, total, summed = lax.cond(
        jnp.int32(0) <= own_start,
        update,
        lambda state: state,
        (best_start, total_start, summed_start),
    )
    attended = summed.reshape(seq_rows, local_heads, group, head_size) / total[..., None]
    attended = attended.astype(jnp.bfloat16).reshape(seq_rows, local_heads * group * head_size)
    by_position = lax.all_to_all(attended, "tp", split_axis=0, concat_axis=1, tiled=True)
    return jnp.dot(by_position, out_weight, preferred_element_type=jnp.float32).astype(jnp.bfloat16)


def expert_half(routed_input, norm_gain, routes, route_weight, expert_gate, expert_up, expert_down):
    group_size = lax.axis_size("tp")
    ep_size = lax.axis_size("ep")
    tp_index = lax.axis_index("tp")
    seq_rows, width = routed_input.shape
    own_rows = seq_rows // group_size
    local_experts = expert_gate.shape[0]
    expert_count = local_experts * ep_size
    top_count = routes.shape[1]
    capacity = max(2, own_rows * top_count * 3 // (2 * expert_count))
    per_device = local_experts * capacity
    mine = lax.dynamic_slice_in_dim(routed_input, tp_index * own_rows, own_rows, 0)
    own_routes = lax.dynamic_slice_in_dim(routes, tp_index * own_rows, own_rows, 0)
    chooser = slot_chooser(own_routes, expert_count, capacity)
    normed = rms_rows(mine, norm_gain)
    outgoing = jnp.einsum("tks,td->sd", chooser, normed, preferred_element_type=jnp.float32).astype(
        jnp.bfloat16
    )
    arrived = lax.all_to_all(
        outgoing.reshape(1, ep_size, per_device, width),
        "ep",
        split_axis=1,
        concat_axis=1,
        tiled=True,
    )
    received = lax.all_gather(arrived, "tp", axis=0, tiled=True)
    blocks = received.shape[0]
    divide_point = received.reshape(blocks, ep_size, local_experts, capacity, width)
    gate = jnp.einsum(
        "abecd,edf->abecf", divide_point, expert_gate, preferred_element_type=jnp.float32
    )
    upper = jnp.einsum(
        "abecd,edf->abecf", divide_point, expert_up, preferred_element_type=jnp.float32
    )
    hidden = (jax.nn.silu(gate) * upper).astype(jnp.bfloat16)
    partial_value = jnp.einsum(
        "abecf,efd->abecd", hidden, expert_down, preferred_element_type=jnp.float32
    )
    rounded = lax.optimization_barrier(partial_value.astype(jnp.bfloat16)).astype(jnp.float32)
    summed = lax.psum_scatter(
        rounded.reshape(lax.axis_size("tp") * 1, ep_size, per_device, width).astype(jnp.bfloat16),
        "tp",
        scatter_dimension=0,
        tiled=True,
    )
    returned = lax.all_to_all(summed, "ep", split_axis=1, concat_axis=1, tiled=True)
    picked = jnp.einsum(
        "tks,sd->tkd",
        chooser,
        returned.reshape(ep_size * per_device, width),
        preferred_element_type=jnp.float32,
    )
    own_weight = lax.dynamic_slice_in_dim(route_weight, tp_index * own_rows, own_rows, 0)
    return jnp.sum(own_weight[:, :, None] * picked, axis=1).astype(jnp.bfloat16)


def body(
    queries,
    key_cache,
    value_cache,
    cum_gate,
    out_weight,
    routed_input,
    norm_gain,
    routes,
    route_weight,
    expert_gate,
    expert_up,
    expert_down,
):
    mixed_out = mixer_half(queries, key_cache, value_cache, cum_gate, out_weight)
    expert_out = expert_half(
        routed_input, norm_gain, routes, route_weight, expert_gate, expert_up, expert_down
    )
    return (mixed_out, expert_out)


def solution(mesh):
    return jax.shard_map(
        body,
        mesh=mesh,
        in_specs=(
            P("ep", "tp"),
            P("tp", None, "ep"),
            P("tp", None, "ep"),
            P("tp", None),
            P(),
            P("ep", None),
            P(),
            P("ep", None),
            P("ep", None),
            P("ep", None, "tp"),
            P("ep", None, "tp"),
            P("ep", "tp", None),
        ),
        out_specs=(P(("ep", "tp"), None), P(("ep", "tp"), None)),
        check_vma=False,
    )
```

profile of v0, /device:TPU:0, one launch (start us, length us, event | category | flops | bytes accessed | tf_op | source)
XLA Modules:
  0.0 172.3 jit_solution(1201821751376832034)
XLA Ops:
  7.2 0.0 copy-start
  7.2 0.0 copy-start.5
  7.2 0.0 all-gather.2.cloned.1.call-start
  7.2 0.9 constant_dynamic-slice_fusion
  8.2 0.1 copy.56
  8.3 0.1 eq.51
  8.4 0.1 fusion.36
  8.5 0.2 reduce_window_sum.11
  8.7 0.2 select_reduce_fusion
  8.9 0.1 reduce_sum.48
  9.0 0.1 copy.57
  9.1 0.8 multiply_add_fusion
  9.8 0.1 convert_reduce_fusion
  9.9 1.1 fusion.23
  11.1 0.7 convert_element_type.68
  11.8 1.4 convolution_convert_fusion.1
  13.1 27.4 %all_to_all.29 = bf16[1,8,24,2048]{3,2,0,1:T(8,128)(2,1)} all-to-all(bf16[1,8,24,2048]{3,2,0,1:T(8,128)(2,1)S(1)} %bitcast.129), channel_id=1, replica_groups=mesh['ep'=8,'tp'=4] {'ep'}, dimensions={1} | all-to-all | bytes 1572864 | tf_op jit(solution)/shard_map/all_to_all | solution.py:98
  40.5 0.0 all-gather.2.cloned.1.call-update
  40.5 0.0 reduce-scatter.2.cloned.1.call-start
  40.6 27.6 %all-gather.2.cloned.1.call-done = bf16[4,8,24,2048]{3,2,1,0:T(8,128)(2,1)} async-done(((bf16[1,8,24,2048]{3,2,1,0:T(8,128)(2,1)}), bf16[4,8,24,2048]{3,2,1,0:T(8,128)(2,1)}) %all-gather.2.cloned.1.call-update) | async-done | bytes 3145744 | tf_op jit(solution)/shard_map/all_gather | solution.py:105
  68.2 0.0 copy-done.5
  68.2 3.8 %convolution_bitcast_fusion.2 = f32[4,8,1,24,256]{4,3,1,0,2:T(8,128)} fusion(bf16[4,8,24,2048]{3,2,1,0:T(8,128)(2,1)} %all-gather.2.cloned.1.call-done, bf16[1,2048,256]{2,1,0:T(8,128)(2,1)S(1)} %copy-done.5), kind=kOutput, calls=%fused_computation.26 | convolution fusion | flops 805306368 | bytes 4980736 | tf_op jit(solution)/shard_map/abecd,edf->abecf/dot_general | solution.py:108
  72.0 7.9 %fusion.13 = bf16[4,8,1,24,2048]{4,3,1,0,2:T(8,128)(2,1)} fusion(bf16[1,256,2048]{2,1,0:T(8,128)(2,1)} %param.25, bf16[4,8,24,2048]{3,2,1,0:T(8,128)(2,1)} %all-gather.2.cloned.1.call-done, bf16[1,2048,256]{2,1,0:T(8,128)(2,1)} %param.24, f32[4,8,1,24,256]{4,3,1,0,2:T(8,128)} %convolution_bitcast_fusion.2), kind=kOutput, calls=%fused_computation.21 | convolution fusion | flops 1613365248 | bytes 9175040 | tf_op jit(solution)/shard_map/abecf,efd->abecd/dot_general | solution.py:115
  79.8 0.0 copy-start.2
  79.8 0.0 reduce-scatter.2.cloned.1.call-update
  79.9 0.7 copy-done.2
  80.6 26.2 %all_gather.10 = bf16[1,64,1024]{2,1,0:T(8,128)(2,1)S(1)} all-gather(bf16[1,64,128]{2,1,0:T(8,128)(2,1)S(1)} %copy-done.2), channel_id=1, replica_groups=mesh['ep'=8,'tp'=4] {'ep'}, dimensions={2}, use_global_device_ids=true | all-gather | bytes 147456 | tf_op jit(solution)/shard_map/all_gather | solution.py:40
  106.7 0.0 copy-done.3
  106.7 26.2 %all_gather.9 = bf16[1,64,1024]{2,1,0:T(8,128)(2,1)S(1)} all-gather(bf16[1,64,128]{2,1,0:T(8,128)(2,1)S(1)} %copy-done.3), channel_id=1, replica_groups=mesh['ep'=8,'tp'=4] {'ep'}, dimensions={2}, use_global_device_ids=true | all-gather | bytes 147456 | tf_op jit(solution)/shard_map/all_gather | solution.py:39
  132.9 0.0 copy-done.1
  132.9 0.0 copy-done.6
  132.9 0.0 copy-start.4
  132.9 1.2 conditional.1
  132.9 0.1 dynamic-slice_bitcast_fusion
  133.0 0.1 iota_compare_fusion
  133.1 0.1 copy.53
  133.2 0.4 fusion.41
  133.7 0.2 fusion.7
  133.8 0.3 fusion.5
  134.2 0.1 copy.54
  134.3 6.3 %all_to_all.30 = bf16[4,32,128]{2,1,0:T(8,128)(2,1)S(1)} all-to-all(bf16[4,32,128]{2,1,0:T(8,128)(2,1)S(1)} %bitcast.133), channel_id=1, replica_groups=mesh['ep'=8,'tp'=4] {'tp'}, dimensions={0} | all-to-all | bytes 65536 | tf_op jit(solution)/shard_map/all_to_all | solution.py:76
  140.6 3.5 %all-to-all-start.2 = ((bf16[1,8,24,2048]{3,2,0,1:T(8,128)(2,1)}), bf16[1,8,24,2048]{3,2,0,1:T(8,128)(2,1)S(1)}, u32[]{:S(2)}, u32[]{:S(2)}) async-start(bf16[1,8,24,2048]{3,2,0,1:T(8,128)(2,1)} %bitcast.130), calls=%async_computation.3 | async-start | bytes 1572864 | tf_op jit(solution)/shard_map/all_to_all | solution.py:125
  144.1 0.0 copy-done.4
  144.1 0.1 constant_dynamic-slice_fusion.1
  144.2 0.0 copy-done
  144.2 1.1 convolution_convert_fusion.2
  145.4 19.1 %all-to-all-done.2 = bf16[1,8,24,2048]{3,2,0,1:T(8,128)(2,1)S(1)} async-done(((bf16[1,8,24,2048]{3,2,0,1:T(8,128)(2,1)}), bf16[1,8,24,2048]{3,2,0,1:T(8,128)(2,1)S(1)}, u32[]{:S(2)}, u32[]{:S(2)}) %all-to-all-start.2) | async-done | bytes 786464 | tf_op jit(solution)/shard_map/all_to_all | solution.py:125
  164.4 1.1 fusion.15
  (9 shorter events, 0.0 us)
Async XLA Ops:
  7.2 137.1 %copy-start = (bf16[512,2048]{1,0:T(8,128)(2,1)S(1)}, bf16[512,2048]{1,0:T(8,128)(2,1)}, u32[]{:S(2)}) copy-start(bf16[512,2048]{1,0:T(8,128)(2,1)} %param.18) | copy-start | bytes 6291460
  7.2 61.0 %copy-start.5 = (bf16[1,2048,256]{2,1,0:T(8,128)(2,1)S(1)}, bf16[1,2048,256]{2,1,0:T(8,128)(2,1)}, u32[]{:S(2)}) copy-start(bf16[1,2048,256]{2,1,0:T(8,128)(2,1)} %param.23) | copy-start | bytes 3145732
  7.2 61.0 %all-gather.2.cloned.1.call-start = ((), (), s32[]{:S(2)}) async-start(), calls=%async_computation.4 | async-start | bytes 3932160 | tf_op jit(solution)/shard_map/all_gather | solution.py:105
  40.5 100.0 %reduce-scatter.2.cloned.1.call-start = ((), (), s32[]{:S(2)}) async-start(), calls=%async_computation.5 | async-start | bytes 3932160 | tf_op jit(solution)/shard_map/reduce_scatter | solution.py:119
  79.8 0.7 copy-start.2
  79.8 26.9 %copy-start.3 = (bf16[1,64,128]{2,1,0:T(8,128)(2,1)S(1)}, bf16[1,64,128]{2,1,0:T(8,128)(2,1)}, u32[]{:S(2)}) copy-start(bf16[1,64,128]{2,1,0:T(8,128)(2,1)} %param.15) | copy-start | bytes 49156
  79.8 53.1 %copy-start.1 = (bf16[128,128]{1,0:T(8,128)(2,1)S(1)}, bf16[128,128]{1,0:T(8,128)(2,1)}, u32[]{:S(2)}) copy-start(bf16[128,128]{1,0:T(8,128)(2,1)} %param.14) | copy-start | bytes 98308
  79.8 53.1 %copy-start.6 = (f32[1,1024]{1,0:T(1,128)S(1)}, f32[1,1024]{1,0:T(1,128)}, u32[]{:S(2)}) copy-start(f32[1,1024]{1,0:T(1,128)} %param.17) | copy-start | bytes 12292
  132.9 11.2 %copy-start.4 = (f32[256,2]{0,1:T(2,128)S(1)}, f32[256,2]{0,1:T(2,128)}, u32[]{:S(2)}) copy-start(f32[256,2]{0,1:T(2,128)} %param.22) | copy-start | bytes 6148
  140.6 23.8 %all-to-all-start.2 = ((bf16[1,8,24,2048]{3,2,0,1:T(8,128)(2,1)}), bf16[1,8,24,2048]{3,2,0,1:T(8,128)(2,1)S(1)}, u32[]{:S(2)}, u32[]{:S(2)}) async-start(bf16[1,8,24,2048]{3,2,0,1:T(8,128)(2,1)} %bitcast.130), calls=%async_computation.3 | async-start | bytes 1572864 | tf_op jit(solution)/shard_map/all_to_all | solution.py:125
Sparse Core Ops, SparseCore 0:
  40.6 27.5 all-gather.1
  80.0 37.8 reduce-scatter.1
where the time goes:
time: 173 us; the launch traced here: 172 us
  blocking collectives  86 us (50%)
  waiting for transfers between devices  46.7 us (27%)
  matrix products  15.9 us (9%)
  between operations  14.2 us (8%)
  starting transfers between devices  3.63 us (2%)
  other arithmetic  3.38 us (2%)
  local copies, waits for them, and re-layouts  2.47 us (1%)
    all_gather x1, waiting for transfers between devices, expert_half(): received = lax.all_gather(arrived, 'tp', axis=0, tiled=True)  27.6 us
    all_to_all x1, blocking collectives, expert_half(): lax.all_to_all(outgoing.reshape(1, ep_size, per_device, width), 'ep', spl...  27.4 us
    all_gather x1, blocking collectives, mixer_half(): lax.all_gather(value_cache, 'ep', axis=2, tiled=True)  26.2 us
    all_gather x1, blocking collectives, mixer_half(): lax.all_gather(key_cache, 'ep', axis=2, tiled=True)  26.2 us
    all_to_all x1, waiting for transfers between devices, expert_half(): lax.all_to_all(summed, 'ep', split_axis=1, concat_axis=1, tiled=True)  19.1 us
    dot_general x1, matrix products, expert_half(): jnp.einsum('abecf,efd->abecd', hidden, expert_down, preferred_element_typ...  7.85 us
    all_to_all x1, blocking collectives, mixer_half(): lax.all_to_all(attended, 'tp', split_axis=0, concat_axis=1, tiled=True)  6.3 us
    dot_general x1, matrix products, expert_half(): jnp.einsum('abecd,edf->abecf', divide_point, expert_gate, preferred_eleme...  3.78 us
  transfers between devices with their start and end apart: 3, of which 2 were waited for; matrix products, arithmetic and copies ran while one was open for 1% of the time, Pallas kernels for 0%

commit v1 on v0

--- a/solution.py
+++ b/solution.py
@@ -1,7 +1,486 @@
+import functools
+
 import jax
 import jax.numpy as jnp
 from jax import lax
+from jax.experimental import pallas as pl
+from jax.experimental.pallas import tpu as pltpu
 from jax.sharding import PartitionSpec as P
+
+MESH = pl.DeviceIdType.MESH
+
+
+def fused_kernel(
+    n,
+    tpn,
+    cap,
+    q_ref,
+    gate_ref,
+    gain_ref,
+    routes_ref,
+    rw_ref,
+    k_any,
+    v_any,
+    ow_any,
+    x_any,
+    wg_any,
+    wu_any,
+    wd_any,
+    mixed_ref,
+    out_ref,
+    xbuf,
+    wgv,
+    wuv,
+    wdv,
+    owv,
+    kv,
+    att,
+    attr,
+    sel,
+    sbuf,
+    recv,
+    part,
+    r1,
+    s2,
+    r2,
+    s3,
+    rbuf,
+    lsem,
+    kvs,
+    kvr,
+    ats,
+    atr,
+    a_s,
+    a_r,
+    bx_s,
+    bx_r,
+    bc_s,
+    bc_r,
+    c_s,
+    c_r,
+    r1_s,
+    r1_r,
+    r2_s,
+    r2_r,
+    r3_s,
+    r3_r,
+):
+    e = lax.axis_index("ep")
+    t = lax.axis_index("tp")
+    partner = t + 1 - 2 * lax.rem(t, 2)
+    peer = lax.rem(t + 2, tpn)
+    opp = lax.rem(partner + 2, tpn)
+    mate = e + 1 - 2 * lax.rem(e, 2)
+    half = n // 2
+    own_rows, width = xbuf.shape
+    wide = width // 2
+    head = k_any.shape[1]
+    seq = q_ref.shape[0]
+
+    barrier = pltpu.get_barrier_semaphore()
+    for s in range(1, n):
+        pl.semaphore_signal(
+            barrier, inc=1, device_id={"ep": lax.rem(e + s, n), "tp": t}, device_id_type=MESH
+        )
+    for s in range(1, tpn):
+        pl.semaphore_signal(
+            barrier, inc=1, device_id={"ep": e, "tp": lax.rem(t + s, tpn)}, device_id_type=MESH
+        )
+
+    load_x = pltpu.make_async_copy(x_any.at[pl.ds(t * own_rows, own_rows)], xbuf, lsem.at[0])
+    load_k = pltpu.make_async_copy(k_any.at[0], kv.at[e, pl.ds(0, head)], lsem.at[1])
+    load_v = pltpu.make_async_copy(v_any.at[0], kv.at[e, pl.ds(head, head)], lsem.at[2])
+    load_g = pltpu.make_async_copy(wg_any.at[0], wgv, lsem.at[3])
+    load_u = pltpu.make_async_copy(wu_any.at[0], wuv, lsem.at[4])
+    load_d = pltpu.make_async_copy(wd_any.at[0], wdv, lsem.at[5])
+    load_o = pltpu.make_async_copy(ow_any, owv, lsem.at[6])
+    load_k.start()
+    load_v.start()
+    load_x.start()
+    load_g.start()
+    load_u.start()
+    load_d.start()
+    load_o.start()
+
+    def remote(src, dst, ssem, rsem, ep, tp):
+        return pltpu.make_async_remote_copy(
+            src_ref=src,
+            dst_ref=dst,
+            send_sem=ssem,
+            recv_sem=rsem,
+            device_id={"ep": ep, "tp": tp},
+            device_id_type=MESH,
+        )
+
+    def kv_far(s):
+        return remote(kv.at[e], kv.at[e], kvs.at[s], kvr.at[s], lax.rem(e + 2 * s, n), t)
+
+    def kv_far_in(s):
+        src = lax.rem(e - 2 * s + n, n)
+        return remote(kv.at[src], kv.at[src], kvs.at[s], kvr.at[s], lax.rem(e + 2 * s, n), t)
+
+    def kv_mate(s):
+        src = lax.rem(e - 2 * s + n, n)
+        return remote(kv.at[src], kv.at[src], kvs.at[half + s], kvr.at[half + s], mate, t)
+
+    def kv_mate_in(s):
+        src = lax.rem(mate - 2 * s + n, n)
+        return remote(kv.at[src], kv.at[src], kvs.at[half + s], kvr.at[half + s], mate, t)
+
+    def source(s):
+        return lax.rem(e - s + n, n)
+
+    def send_a(s):
+        dst = lax.rem(e + s, n)
+        return remote(sbuf.at[dst], recv.at[e, t], a_s.at[s], a_r.at[s], dst, t)
+
+    def copy_a(s):
+        src = source(s)
+        return remote(sbuf.at[src], recv.at[src, t], a_s.at[s], a_r.at[s], lax.rem(e + s, n), t)
+
+    def copy_bx(s, col):
+        src = source(s)
+        return remote(recv.at[src, col], recv.at[src, col], bx_s.at[s], bx_r.at[s], e, peer)
+
+    def copy_bc(s, col):
+        src = source(s)
+        return remote(recv.at[src, col], recv.at[src, col], bc_s.at[s], bc_r.at[s], e, partner)
+
+    def copy_c(s, col):
+        src = source(s)
+        return remote(recv.at[src, col], recv.at[src, col], c_s.at[s], c_r.at[s], e, partner)
+
+    def copy_r1(s, which, col):
+        src = source(s)
+        return remote(
+            part.at[src, col], r1.at[src, which], r1_s.at[s, which], r1_r.at[s, which], e, partner
+        )
+
+    def copy_r2(s):
+        src = source(s)
+        return remote(s2.at[src], r2.at[src], r2_s.at[s], r2_r.at[s], e, peer)
+
+    def copy_r3(s):
+        src = source(s)
+        return remote(s3.at[src], rbuf.at[e], r3_s.at[s], r3_r.at[s], src, t)
+
+    def copy_r3_in(s):
+        src = lax.rem(e + s, n)
+        return remote(s3.at[src], rbuf.at[src], r3_s.at[s], r3_r.at[s], source(s), t)
+
+    load_k.wait()
+    load_v.wait()
+    pl.semaphore_wait(barrier, n - 1 + tpn - 1)
+    for s in range(1, half):
+        kv_far(s).start()
+    kv_mate(0).start()
+
+    lanes = 2 * n * cap
+    place = lax.broadcasted_iota(jnp.int32, (own_rows, lanes), 1).astype(jnp.float32) + 0.5
+    expert = jnp.floor(place / (2.0 * cap))
+    inside = place - 0.5 - expert * (2.0 * cap)
+    right = inside >= cap
+    slot = jnp.where(right, inside - cap, inside)
+    rows = routes_ref[pl.ds(pl.multiple_of(t * own_rows, own_rows), own_rows), :].astype(jnp.float32)
+    top = rows.shape[1]
+    named = [rows[:, k : k + 1] == expert for k in range(top)]
+    total = sum([m.astype(jnp.float32) for m in named])
+    before = lax.broadcasted_iota(jnp.int32, (own_rows, own_rows), 1) < lax.broadcasted_iota(
+        jnp.int32, (own_rows, own_rows), 0
+    )
+    rank = jnp.dot(
+        before.astype(jnp.bfloat16), total.astype(jnp.bfloat16), preferred_element_type=jnp.float32
+    )
+    hit = rank == slot
+    chosen = jnp.where(hit, total, 0.0)
+    for k in range(top):
+        mine = jnp.where(hit & named[k], 1.0, 0.0)
+        sel[2 * k * own_rows : (2 * k + 1) * own_rows, :] = jnp.where(right, 0.0, mine).astype(
+            jnp.bfloat16
+        )
+        sel[(2 * k + 1) * own_rows : (2 * k + 2) * own_rows, :] = jnp.where(
+            right, mine, 0.0
+        ).astype(jnp.bfloat16)
+    spread = jnp.concatenate(
+        [jnp.where(right, 0.0, chosen), jnp.where(right, chosen, 0.0)], axis=0
+    )
+    spread = spread.T.astype(jnp.bfloat16)
+    load_x.wait()
+    x = xbuf[...].astype(jnp.float32)
+    scale = lax.rsqrt(jnp.mean(x * x, axis=-1, keepdims=True) + 1e-06)
+    normed = (x * scale * gain_ref[...].astype(jnp.float32)).astype(jnp.bfloat16)
+    stacked = jnp.concatenate([normed[:, :wide], normed[:, wide:]], axis=0)
+    outgoing = jnp.dot(spread, stacked, preferred_element_type=jnp.float32)
+    sbuf[...] = outgoing.astype(jnp.bfloat16).reshape(sbuf.shape)
+    for s in range(1, n):
+        send_a(s).start()
+    keep = pltpu.make_async_copy(sbuf.at[e], recv.at[e, t], lsem.at[7])
+    keep.start()
+    keep.wait()
+    copy_bx(0, t).start()
+    copy_bc(0, t).start()
+
+    for s in range(1, half):
+        kv_far_in(s).wait_recv()
+        kv_mate(s).start()
+    for s in range(half):
+        kv_mate_in(s).wait_recv()
+    own_gate = gate_ref[:, pl.ds(pl.multiple_of(e * seq, seq), seq)]
+    eye = lax.broadcasted_iota(jnp.int32, (seq, seq), 0) == lax.broadcasted_iota(
+        jnp.int32, (seq, seq), 1
+    )
+    gate_col = jnp.sum(
+        jnp.where(eye, jnp.broadcast_to(own_gate, (seq, seq)), 0.0), axis=1, keepdims=True
+    )
+    key_pos = lax.broadcasted_iota(jnp.int32, (seq, n * seq), 1)
+    query_pos = lax.broadcasted_iota(jnp.int32, (seq, n * seq), 0) + e * seq
+    bias = gate_col - gate_ref[...]
+    group = q_ref.shape[1] // head
+    heads_out = []
+    for g in range(group):
+        q = q_ref[:, g * head : (g + 1) * head]
+        scores = jnp.concatenate(
+            [
+                jnp.dot(q, kv[j, 0:head, :], preferred_element_type=jnp.float32)
+                for j in range(n)
+            ],
+            axis=1,
+        )
+        scores = scores * (head ** (-0.5)) + bias
+        scores = jnp.where(key_pos <= query_pos, scores, -jnp.inf)
+        weights = jnp.exp(scores - jnp.max(scores, axis=-1, keepdims=True))
+        whole = jnp.sum(weights, axis=-1, keepdims=True)
+        weights = weights.astype(jnp.bfloat16)
+        summed = jnp.zeros((seq, head), jnp.float32)
+        for j in range(n):
+            summed = summed + lax.dot_general(
+                weights[:, j * seq : (j + 1) * seq],
+                kv[j, head : 2 * head, :],
+                (((1,), (1,)), ((), ())),
+                preferred_element_type=jnp.float32,
+            )
+        heads_out.append(summed / whole)
+    attended = jnp.concatenate(heads_out, axis=1).astype(jnp.bfloat16)
+    att[...] = attended.reshape(att.shape)
+    attr[t] = att[t]
+
+    def copy_att(s):
+        dst = lax.rem(t + s, tpn)
+        return remote(att.at[dst], attr.at[t], ats.at[s], atr.at[s], e, dst)
+
+    def copy_att_in(s):
+        src = lax.rem(t - s + tpn, tpn)
+        return remote(att.at[src], attr.at[src], ats.at[s], atr.at[s], e, lax.rem(t + s, tpn))
+
+    for s in range(1, tpn):
+        copy_att(s).start()
+    load_g.wait()
+    load_u.wait()
+    load_d.wait()
+
+    def step(i, carry):
+        @pl.when((i >= 1) & (i < n))
+        def _():
+            copy_a(i).wait_recv()
+            copy_bx(i, t).start()
+            copy_bc(i, t).start()
+
+        @pl.when((i >= 1) & (i <= n))
+        def _():
+            copy_bx(i - 1, peer).wait_recv()
+            copy_c(i - 1, peer).start()
+
+        @pl.when((i >= 2) & (i <= n + 1))
+        def _():
+            s = i - 2
+            src = source(s)
+            copy_bc(s, partner).wait_recv()
+            copy_c(s, opp).wait_recv()
+            block = recv[src].astype(jnp.float32)
+            count = block.shape[0] * cap
+            lo = block[:, :cap].reshape(count, wide).astype(jnp.bfloat16)
+            hi = block[:, cap:].reshape(count, wide).astype(jnp.bfloat16)
+            gate = jnp.dot(lo, wgv[0:wide, :], preferred_element_type=jnp.float32) + jnp.dot(
+                hi, wgv[wide:, :], preferred_element_type=jnp.float32
+            )
+            upper = jnp.dot(lo, wuv[0:wide, :], preferred_element_type=jnp.float32) + jnp.dot(
+                hi, wuv[wide:, :], preferred_element_type=jnp.float32
+            )
+            hidden = (gate / (1.0 + jnp.exp(-gate)) * upper).astype(jnp.bfloat16)
+            down = jnp.dot(hidden, wdv[...], preferred_element_type=jnp.float32)
+            shape = (tpn, cap, wide)
+            part[src] = jnp.concatenate(
+                [down[:, :wide].reshape(shape), down[:, wide:].reshape(shape)], axis=1
+            ).astype(jnp.bfloat16)
+            copy_r1(s, 1, opp).start()
+            copy_r1(s, 0, partner).start()
+
+        @pl.when((i >= 3) & (i <= n + 2))
+        def _():
+            s = i - 3
+            src = source(s)
+            copy_r1(s, 1, opp).wait_recv()
+            copy_r1(s, 0, partner).wait_recv()
+            s2[src] = (
+                part[src, peer].astype(jnp.float32) + r1[src, 1].astype(jnp.float32)
+            ).astype(jnp.bfloat16)
+            copy_r2(s).start()
+
+        @pl.when(i >= 4)
+        def _():
+            s = i - 4
+            src = source(s)
+            copy_r2(s).wait_recv()
+            s3[src] = (
+                part[src, t].astype(jnp.float32)
+                + r1[src, 0].astype(jnp.float32)
+                + r2[src].astype(jnp.float32)
+            ).astype(jnp.bfloat16)
+
+            @pl.when(s > 0)
+            def _():
+                copy_r3(s).start()
+
+            @pl.when(s == 0)
+            def _():
+                rbuf[e] = s3[e]
+
+        return carry
+
+    lax.fori_loop(1, n + 4, step, 0)
+
+    for s in range(1, tpn):
+        copy_att_in(s).wait_recv()
+    load_o.wait()
+    joined = jnp.concatenate([attr[j] for j in range(tpn)], axis=1)
+    mixed_ref[...] = jnp.dot(joined, owv[...], preferred_element_type=jnp.float32).astype(
+        jnp.bfloat16
+    )
+
+    for s in range(1, n):
+        copy_r3_in(s).wait_recv()
+    picked = jnp.dot(
+        sel[...], rbuf[...].reshape(lanes, wide), preferred_element_type=jnp.float32
+    )
+    rw = rw_ref[pl.ds(pl.multiple_of(t * own_rows, own_rows), own_rows), :]
+    for h in range(2):
+        acc = jnp.zeros((own_rows, wide), jnp.float32)
+        for k in range(top):
+            at = (2 * k + h) * own_rows
+            acc = acc + rw[:, k : k + 1] * picked[at : at + own_rows]
+        out_ref[:, h * wide : (h + 1) * wide] = acc.astype(jnp.bfloat16)
+
+    for s in range(1, half):
+        kv_far(s).wait_send()
+    for s in range(half):
+        kv_mate(s).wait_send()
+    for s in range(1, tpn):
+        copy_att(s).wait_send()
+
+    def drain(s, carry):
+        copy_bx(s, t).wait_send()
+        copy_bc(s, t).wait_send()
+        copy_c(s, peer).wait_send()
+        copy_r1(s, 0, partner).wait_send()
+        copy_r1(s, 1, opp).wait_send()
+        copy_r2(s).wait_send()
+
+        @pl.when(s > 0)
+        def _():
+            send_a(s).wait_send()
+            copy_r3(s).wait_send()
+
+        return carry
+
+    lax.fori_loop(0, n, drain, 0)
+
+
+def fused_body(
+    n,
+    tpn,
+    queries,
+    key_cache,
+    value_cache,
+    cum_gate,
+    out_weight,
+    routed_input,
+    norm_gain,
+    routes,
+    route_weight,
+    expert_gate,
+    expert_up,
+    expert_down,
+):
+    seq = queries.shape[0]
+    head = key_cache.shape[1]
+    width = routed_input.shape[1]
+    wide = width // 2
+    own_rows = routed_input.shape[0] // tpn
+    top = routes.shape[1]
+    units = expert_gate.shape[2]
+    cap = block_capacity(own_rows, top, n * expert_gate.shape[0])
+    bf16 = jnp.bfloat16
+    chunk = (2 * cap, wide)
+    vmem = pl.BlockSpec(memory_space=pltpu.VMEM)
+    anywhere = pl.BlockSpec(memory_space=pl.ANY)
+    dma = pltpu.SemaphoreType.DMA
+    mixed, out = pl.pallas_call(
+        functools.partial(fused_kernel, n, tpn, cap),
+        out_shape=(
+            jax.ShapeDtypeStruct((seq // tpn, width), bf16),
+            jax.ShapeDtypeStruct((own_rows, width), bf16),
+        ),
+        in_specs=[vmem] * 5 + [anywhere] * 7,
+        out_specs=(vmem, vmem),
+        scratch_shapes=[
+            pltpu.VMEM((own_rows, width), bf16),
+            pltpu.VMEM((width, units), bf16),
+            pltpu.VMEM((width, units), bf16),
+            pltpu.VMEM((units, width), bf16),
+            pltpu.VMEM(out_weight.shape, bf16),
+            pltpu.VMEM((n, 2 * head, seq), bf16),
+            pltpu.VMEM((tpn, seq // tpn, queries.shape[1]), bf16),
+            pltpu.VMEM((tpn, seq // tpn, queries.shape[1]), bf16),
+            pltpu.VMEM((2 * top * own_rows, 2 * n * cap), bf16),
+            pltpu.VMEM((n,) + chunk, bf16),
+            pltpu.VMEM((n, tpn) + chunk, bf16),
+            pltpu.VMEM((n, tpn) + chunk, bf16),
+            pltpu.VMEM((n, 2) + chunk, bf16),
+            pltpu.VMEM((n,) + chunk, bf16),
+            pltpu.VMEM((n,) + chunk, bf16),
+            pltpu.VMEM((n,) + chunk, bf16),
+            pltpu.VMEM((n,) + chunk, bf16),
+            dma((8,)),
+            dma((n,)),
+            dma((n,)),
+            dma((tpn,)),
+            dma((tpn,)),
+        ]
+        + [dma((n,))] * 8
+        + [dma((n, 2))] * 2
+        + [dma((n,))] * 4,
+        compiler_params=pltpu.CompilerParams(
+            collective_id=0, has_side_effects=True, vmem_limit_bytes=48 * 1024 * 1024
+        ),
+    )(
+        queries,
+        cum_gate,
+        norm_gain.reshape(1, width),
+        routes,
+        route_weight,
+        key_cache,
+        value_cache,
+        out_weight,
+        routed_input,
+        expert_gate,
+        expert_up,
+        expert_down,
+    )
+    return mixed, out
+
+
+def block_capacity(own_rows, top_count, expert_count):
+    return max(2, own_rows * top_count * 3 // (2 * expert_count))
 
 
 def slot_chooser(route_rows, expert_count, capacity):
@@ -154,9 +633,50 @@
     return (mixed_out, expert_out)
 
 
+def pick_body(
+    n,
+    tpn,
+    queries,
+    key_cache,
+    value_cache,
+    cum_gate,
+    out_weight,
+    routed_input,
+    norm_gain,
+    routes,
+    route_weight,
+    expert_gate,
+    *rest,
+):
+    seq, columns = queries.shape
+    own_rows = routed_input.shape[0] // tpn
+    cap = block_capacity(own_rows, routes.shape[1], n * expert_gate.shape[0])
+    fits = (
+        tpn == 4
+        and n % 2 == 0
+        and cap % 8 == 0
+        and expert_gate.shape[0] == 1
+        and key_cache.shape[0] == 1
+        and seq % 128 == 0
+    )
+    args = (
+        queries,
+        key_cache,
+        value_cache,
+        cum_gate,
+        out_weight,
+        routed_input,
+        norm_gain,
+        routes,
+        route_weight,
+        expert_gate,
+    ) + rest
+    return fused_body(n, tpn, *args) if fits else body(*args)
+
+
 def solution(mesh):
     return jax.shard_map(
-        body,
+        functools.partial(pick_body, mesh.shape["ep"], mesh.shape["tp"]),
         mesh=mesh,
         in_specs=(
             P("ep", "tp"),

time: 173 us -> 75.9 us (0.44)
  blocking collectives: 86 us -> 0 us
  Pallas kernels: 0 us -> 63.2 us
  waiting for transfers between devices: 46.7 us -> 0 us
  matrix products: 15.9 us -> 0 us
  between operations: 14.2 us -> 0.67 us
  local copies, waits for them, and re-layouts: 2.47 us -> 11.4 us
  starting transfers between devices: 3.63 us -> 0 us
  other arithmetic: 3.38 us -> 0 us
    pallas_call x0 -> x1, Pallas kernels: none -> 63.2 us  [fused_body(): pl.pallas_call(functools.partial(fused_kernel, n, tpn, cap), out_shape=(j...]
    all_gather x2 -> x0, blocking collectives: 52.4 us -> none  [the longest x1 26.2 us: mixer_half(): lax.all_gather(value_cache, 'ep', axis=2, tiled=True)]
    all_to_all x2 -> x0, blocking collectives: 33.7 us -> none  [the longest x1 27.4 us: expert_half(): lax.all_to_all(outgoing.reshape(1, ep_size, per_device, width), 'ep', spl...]
    all_gather x1 -> x0, waiting for transfers between devices: 27.6 us -> none  [expert_half(): received = lax.all_gather(arrived, 'tp', axis=0, tiled=True)]
    all_to_all x1 -> x0, waiting for transfers between devices: 19.1 us -> none  [expert_half(): lax.all_to_all(summed, 'ep', split_axis=1, concat_axis=1, tiled=True)]
    dot_general x7 -> x0, matrix products: 15.9 us -> none  [the longest x1 7.85 us: expert_half(): jnp.einsum('abecf,efd->abecd', hidden, expert_down, preferred_element_typ...]
    unnamed x14 -> x20, local copies, waits for them, and re-layouts: 0.71 us -> 10.8 us
    all_to_all x1 -> x0, starting transfers between devices: 3.55 us -> none  [expert_half(): lax.all_to_all(summed, 'ep', split_axis=1, concat_axis=1, tiled=True)]
  transfers between devices with their start and end apart: 3 -> 0, of which waited for: 2 -> 0; matrix products, arithmetic and copies ran while one was open for 1% -> 0% of each run, Pallas kernels for 0% -> 0%
where the time goes in v1:
time: 75.9 us; the launch traced here: 75.3 us
  Pallas kernels  63.2 us (83%)
  local copies, waits for them, and re-layouts  11.4 us (15%)
    pallas_call x1, Pallas kernels, fused_body(): pl.pallas_call(functools.partial(fused_kernel, n, tpn, cap), out_shape=(j...  63.2 us
    unnamed x20, local copies, waits for them, and re-layouts  10.8 us

profile of v1, /device:TPU:0, one launch (start us, length us, event | category | flops | bytes accessed | tf_op | source)
XLA Modules:
  0.0 75.3 jit_solution(4885461024495049299)
XLA Ops:
  0.6 0.7 reshape.7.gain_ref
  1.3 0.8 %copy.14.routes_ref = s32[256,2]{1,0:T(8,128)S(1)} copy(s32[256,2]{0,1:T(2,128)} %param.19) | data formatting | bytes 4096 | tf_op args[7]
  2.1 0.8 %copy.15.rw_ref = f32[256,2]{1,0:T(8,128)S(1)} copy(f32[256,2]{0,1:T(2,128)} %param.20) | data formatting | bytes 4096 | tf_op args[8]
  3.0 0.0 copy-start
  3.0 1.2 %copy-done = bf16[256,2048]{1,0:T(8,128)(2,1)S(1)} copy-done((bf16[256,2048]{1,0:T(8,128)(2,1)S(1)}, bf16[256,2048]{1,0:T(8,128)(2,1)}, u32[]{:S(2)}) %copy-start) | copy-done | bytes 1048600
  4.2 0.0 copy-start.1
  4.2 1.2 %copy-done.1 = bf16[1,2048,256]{2,1,0:T(8,128)(2,1)S(1)} copy-done((bf16[1,2048,256]{2,1,0:T(8,128)(2,1)S(1)}, bf16[1,2048,256]{2,1,0:T(8,128)(2,1)}, u32[]{:S(2)}) %copy-start.1) | copy-done | bytes 1048600
  5.4 0.0 copy-start.2
  5.4 1.2 %copy-done.2 = bf16[1,2048,256]{2,1,0:T(8,128)(2,1)S(1)} copy-done((bf16[1,2048,256]{2,1,0:T(8,128)(2,1)S(1)}, bf16[1,2048,256]{2,1,0:T(8,128)(2,1)}, u32[]{:S(2)}) %copy-start.2) | copy-done | bytes 1048600
  6.6 0.0 copy-start.3
  6.6 1.2 %copy-done.3 = bf16[1,256,2048]{2,1,0:T(8,128)(2,1)S(1)} copy-done((bf16[1,256,2048]{2,1,0:T(8,128)(2,1)S(1)}, bf16[1,256,2048]{2,1,0:T(8,128)(2,1)}, u32[]{:S(2)}) %copy-start.3) | copy-done | bytes 1048600
  7.9 0.0 copy-start.4
  7.9 0.8 %copy-done.4 = bf16[128,128]{1,0:T(8,128)(2,1)S(1)} copy-done((bf16[128,128]{1,0:T(8,128)(2,1)S(1)}, bf16[128,128]{1,0:T(8,128)(2,1)}, u32[]{:S(2)}) %copy-start.4) | copy-done | bytes 32792
  8.6 0.0 copy-start.5
  8.6 0.7 copy-done.5
  9.3 0.0 copy-start.6
  9.3 0.7 copy-done.6
  10.1 0.0 copy-start.7
  10.1 0.7 copy-done.7
  10.7 63.2 %shard_map.131 = (bf16[32,2048]{1,0:T(8,128)(2,1)S(1)}, bf16[64,2048]{1,0:T(8,128)(2,1)S(1)}) custom-call(bf16[128,128]{1,0:T(8,128)(2,1)S(1)} %copy-done.4, f32[1,1024]{1,0:T(1,128)S(1)} %copy-done.7, bf16[1,2048]{1,0:T(2,128)(2,1)S(1)} %reshape.7.gain_ref, s32[256,2]{1,0:T(8,128)S(1)} %copy.14.routes_ref, f32[256,2]{1,0:T(8,128)S(1)} %copy.15.rw_ref, ...), custom_call_target="tpu_custom_call" | custom-call | tf_op jit(solution)/shard_map/pallas_call | solution.py:427
  74.0 0.7 copy.18
  74.6 0.7 copy.19
Async XLA Ops:
  3.0 1.2 %copy-start = (bf16[256,2048]{1,0:T(8,128)(2,1)S(1)}, bf16[256,2048]{1,0:T(8,128)(2,1)}, u32[]{:S(2)}) copy-start(bf16[256,2048]{1,0:T(8,128)(2,1)} %x_any.1) | copy-start | bytes 3145732
  4.2 1.2 %copy-start.1 = (bf16[1,2048,256]{2,1,0:T(8,128)(2,1)S(1)}, bf16[1,2048,256]{2,1,0:T(8,128)(2,1)}, u32[]{:S(2)}) copy-start(bf16[1,2048,256]{2,1,0:T(8,128)(2,1)} %wg_any.1) | copy-start | bytes 3145732
  5.4 1.2 %copy-start.2 = (bf16[1,2048,256]{2,1,0:T(8,128)(2,1)S(1)}, bf16[1,2048,256]{2,1,0:T(8,128)(2,1)}, u32[]{:S(2)}) copy-start(bf16[1,2048,256]{2,1,0:T(8,128)(2,1)} %wu_any.1) | copy-start | bytes 3145732
  6.6 1.2 %copy-start.3 = (bf16[1,256,2048]{2,1,0:T(8,128)(2,1)S(1)}, bf16[1,256,2048]{2,1,0:T(8,128)(2,1)}, u32[]{:S(2)}) copy-start(bf16[1,256,2048]{2,1,0:T(8,128)(2,1)} %wd_any.1) | copy-start | bytes 3145732
  7.9 0.8 %copy-start.4 = (bf16[128,128]{1,0:T(8,128)(2,1)S(1)}, bf16[128,128]{1,0:T(8,128)(2,1)}, u32[]{:S(2)}) copy-start(bf16[128,128]{1,0:T(8,128)(2,1)} %q_ref.1) | copy-start | bytes 98308
  8.6 0.7 copy-start.5
  9.3 0.7 copy-start.6
  10.1 0.7 copy-start.7

commit v2 on v1

--- a/solution.py
+++ b/solution.py
@@ -14,11 +14,11 @@
     n,
     tpn,
     cap,
-    q_ref,
-    gate_ref,
-    gain_ref,
-    routes_ref,
-    rw_ref,
+    q_any,
+    gate_any,
+    gain_any,
+    routes_any,
+    rw_any,
     k_any,
     v_any,
     ow_any,
@@ -28,6 +28,11 @@
     wd_any,
     mixed_ref,
     out_ref,
+    q_ref,
+    gate_ref,
+    gain_ref,
+    routes_ref,
+    rw_ref,
     xbuf,
     wgv,
     wuv,
@@ -94,9 +99,19 @@
     load_u = pltpu.make_async_copy(wu_any.at[0], wuv, lsem.at[4])
     load_d = pltpu.make_async_copy(wd_any.at[0], wdv, lsem.at[5])
     load_o = pltpu.make_async_copy(ow_any, owv, lsem.at[6])
+    load_q = pltpu.make_async_copy(q_any, q_ref, lsem.at[8])
+    load_c = pltpu.make_async_copy(gate_any, gate_ref, lsem.at[9])
+    load_n = pltpu.make_async_copy(gain_any, gain_ref, lsem.at[10])
+    load_r = pltpu.make_async_copy(routes_any, routes_ref, lsem.at[11])
+    load_w = pltpu.make_async_copy(rw_any, rw_ref, lsem.at[12])
     load_k.start()
     load_v.start()
     load_x.start()
+    load_r.start()
+    load_n.start()
+    load_w.start()
+    load_q.start()
+    load_c.start()
     load_g.start()
     load_u.start()
     load_d.start()
@@ -181,9 +196,20 @@
     inside = place - 0.5 - expert * (2.0 * cap)
     right = inside >= cap
     slot = jnp.where(right, inside - cap, inside)
-    rows = routes_ref[pl.ds(pl.multiple_of(t * own_rows, own_rows), own_rows), :].astype(jnp.float32)
-    top = rows.shape[1]
-    named = [rows[:, k : k + 1] == expert for k in range(top)]
+    top, share = routes_ref.shape
+    own = lax.broadcasted_iota(jnp.int32, (own_rows, share), 1) == (
+        lax.broadcasted_iota(jnp.int32, (own_rows, share), 0) + t * own_rows
+    )
+
+    def column(line):
+        return jnp.sum(
+            jnp.where(own, jnp.broadcast_to(line, own.shape), 0.0), axis=1, keepdims=True
+        )
+
+    load_r.wait()
+    named = [
+        column(routes_ref[k : k + 1, :].astype(jnp.float32)) == expert for k in range(top)
+    ]
     total = sum([m.astype(jnp.float32) for m in named])
     before = lax.broadcasted_iota(jnp.int32, (own_rows, own_rows), 1) < lax.broadcasted_iota(
         jnp.int32, (own_rows, own_rows), 0
@@ -206,9 +232,12 @@
     )
     spread = spread.T.astype(jnp.bfloat16)
     load_x.wait()
+    load_n.wait()
     x = xbuf[...].astype(jnp.float32)
+    gain = gain_ref[...].astype(jnp.float32)
+    gain = jnp.concatenate([gain[j : j + 1, :] for j in range(gain.shape[0])], axis=1)
     scale = lax.rsqrt(jnp.mean(x * x, axis=-1, keepdims=True) + 1e-06)
-    normed = (x * scale * gain_ref[...].astype(jnp.float32)).astype(jnp.bfloat16)
+    normed = (x * scale * gain).astype(jnp.bfloat16)
     stacked = jnp.concatenate([normed[:, :wide], normed[:, wide:]], axis=0)
     outgoing = jnp.dot(spread, stacked, preferred_element_type=jnp.float32)
     sbuf[...] = outgoing.astype(jnp.bfloat16).reshape(sbuf.shape)
@@ -225,6 +254,8 @@
         kv_mate(s).start()
     for s in range(half):
         kv_mate_in(s).wait_recv()
+    load_q.wait()
+    load_c.wait()
     own_gate = gate_ref[:, pl.ds(pl.multiple_of(e * seq, seq), seq)]
     eye = lax.broadcasted_iota(jnp.int32, (seq, seq), 0) == lax.broadcasted_iota(
         jnp.int32, (seq, seq), 1
@@ -362,12 +393,13 @@
     picked = jnp.dot(
         sel[...], rbuf[...].reshape(lanes, wide), preferred_element_type=jnp.float32
     )
-    rw = rw_ref[pl.ds(pl.multiple_of(t * own_rows, own_rows), own_rows), :]
+    load_w.wait()
+    rw = [column(rw_ref[k : k + 1, :]) for k in range(top)]
     for h in range(2):
         acc = jnp.zeros((own_rows, wide), jnp.float32)
         for k in range(top):
             at = (2 * k + h) * own_rows
-            acc = acc + rw[:, k : k + 1] * picked[at : at + own_rows]
+            acc = acc + rw[k] * picked[at : at + own_rows]
         out_ref[:, h * wide : (h + 1) * wide] = acc.astype(jnp.bfloat16)
 
     for s in range(1, half):
@@ -422,7 +454,7 @@
     bf16 = jnp.bfloat16
     chunk = (2 * cap, wide)
     vmem = pl.BlockSpec(memory_space=pltpu.VMEM)
-    anywhere = pl.BlockSpec(memory_space=pl.ANY)
+    anywhere = pl.BlockSpec(memory_space=pltpu.HBM)
     dma = pltpu.SemaphoreType.DMA
     mixed, out = pl.pallas_call(
         functools.partial(fused_kernel, n, tpn, cap),
@@ -430,9 +462,14 @@
             jax.ShapeDtypeStruct((seq // tpn, width), bf16),
             jax.ShapeDtypeStruct((own_rows, width), bf16),
         ),
-        in_specs=[vmem] * 5 + [anywhere] * 7,
+        in_specs=[anywhere] * 12,
         out_specs=(vmem, vmem),
         scratch_shapes=[
+            pltpu.VMEM(queries.shape, bf16),
+            pltpu.VMEM(cum_gate.shape, jnp.float32),
+            pltpu.VMEM((width // 128, 128), bf16),
+            pltpu.VMEM((top, tpn * own_rows), jnp.int32),
+            pltpu.VMEM((top, tpn * own_rows), jnp.float32),
             pltpu.VMEM((own_rows, width), bf16),
             pltpu.VMEM((width, units), bf16),
             pltpu.VMEM((width, units), bf16),
@@ -450,7 +487,7 @@
             pltpu.VMEM((n,) + chunk, bf16),
             pltpu.VMEM((n,) + chunk, bf16),
             pltpu.VMEM((n,) + chunk, bf16),
-            dma((8,)),
+            dma((13,)),
             dma((n,)),
             dma((n,)),
             dma((tpn,)),
@@ -460,14 +497,14 @@
         + [dma((n, 2))] * 2
         + [dma((n,))] * 4,
         compiler_params=pltpu.CompilerParams(
-            collective_id=0, has_side_effects=True, vmem_limit_bytes=48 * 1024 * 1024
+            collective_id=0, has_side_effects=True, vmem_limit_bytes=60 * 1024 * 1024
         ),
     )(
         queries,
         cum_gate,
-        norm_gain.reshape(1, width),
-        routes,
-        route_weight,
+        norm_gain.reshape(width // 128, 128),
+        routes.T,
+        route_weight.T,
         key_cache,
         value_cache,
         out_weight,

time: 75.9 us -> 68.3 us (0.90)
  local copies, waits for them, and re-layouts: 11.4 us -> 3.24 us
  Pallas kernels: 63.2 us -> 64.2 us
    unnamed x20 -> x2, local copies, waits for them, and re-layouts: 10.8 us -> 3.24 us
    pallas_call x1, Pallas kernels: 63.2 us -> 64.2 us  [fused_body(): pl.pallas_call(functools.partial(fused_kernel, n, tpn, cap), out_shape=(j...]
where the time goes in v2:
time: 68.3 us; the launch traced here: 68.1 us
  Pallas kernels  64.2 us (94%)
  local copies, waits for them, and re-layouts  3.24 us (5%)
    pallas_call x1, Pallas kernels, fused_body(): pl.pallas_call(functools.partial(fused_kernel, n, tpn, cap), out_shape=(j...  64.2 us
    unnamed x2, local copies, waits for them, and re-layouts  3.24 us

profile of v2, /device:TPU:0, one launch (start us, length us, event | category | flops | bytes accessed | tf_op | source)
XLA Modules:
  0.0 68.1 jit_solution(15018533038223685835)
XLA Ops:
  0.6 64.2 %shard_map.131 = (bf16[32,2048]{1,0:T(8,128)(2,1)}, bf16[64,2048]{1,0:T(8,128)(2,1)}) custom-call(bf16[128,128]{1,0:T(8,128)(2,1)} %q_any.1, f32[1,1024]{1,0:T(1,128)} %gate_any.1, bf16[16,128]{1,0:T(8,128)(2,1)} %bitcast.3, s32[2,256]{1,0:T(2,128)} %bitcast.4, f32[2,256]{1,0:T(2,128)} %bitcast.5, bf16[1,64,128]{2,1,0:T(8,128)(2,1)} %k_any.1, ...), custom_call_target="tpu_custom_call" | custom-call | tf_op jit(solution)/shard_map/pallas_call | solution.py:459
  64.9 1.6 %copy.16 = bf16[32,2048]{1,0:T(8,128)(2,1)} copy(bf16[32,2048]{1,0:T(8,128)(2,1)} %get-tuple-element.4) | data formatting | bytes 262144
  66.4 1.7 %copy.17 = bf16[64,2048]{1,0:T(8,128)(2,1)} copy(bf16[64,2048]{1,0:T(8,128)(2,1)} %get-tuple-element.5) | data formatting | bytes 524288

commit v3 on v2

--- a/solution.py
+++ b/solution.py
@@ -43,6 +43,7 @@
     attr,
     sel,
     sbuf,
+    sbuf2,
     recv,
     part,
     r1,
@@ -77,7 +78,7 @@
     opp = lax.rem(partner + 2, tpn)
     mate = e + 1 - 2 * lax.rem(e, 2)
     half = n // 2
-    own_rows, width = xbuf.shape
+    _, own_rows, width = xbuf.shape
     wide = width // 2
     head = k_any.shape[1]
     seq = q_ref.shape[0]
@@ -92,7 +93,10 @@
             barrier, inc=1, device_id={"ep": e, "tp": lax.rem(t + s, tpn)}, device_id_type=MESH
         )
 
-    load_x = pltpu.make_async_copy(x_any.at[pl.ds(t * own_rows, own_rows)], xbuf, lsem.at[0])
+    def load_x(j):
+        at = lax.rem(t + j, tpn) * own_rows
+        return pltpu.make_async_copy(x_any.at[pl.ds(at, own_rows)], xbuf.at[j], lsem.at[12 + j])
+
     load_k = pltpu.make_async_copy(k_any.at[0], kv.at[e, pl.ds(0, head)], lsem.at[1])
     load_v = pltpu.make_async_copy(v_any.at[0], kv.at[e, pl.ds(head, head)], lsem.at[2])
     load_g = pltpu.make_async_copy(wg_any.at[0], wgv, lsem.at[3])
@@ -103,15 +107,17 @@
     load_c = pltpu.make_async_copy(gate_any, gate_ref, lsem.at[9])
     load_n = pltpu.make_async_copy(gain_any, gain_ref, lsem.at[10])
     load_r = pltpu.make_async_copy(routes_any, routes_ref, lsem.at[11])
-    load_w = pltpu.make_async_copy(rw_any, rw_ref, lsem.at[12])
+    load_w = pltpu.make_async_copy(rw_any, rw_ref, lsem.at[0])
     load_k.start()
     load_v.start()
-    load_x.start()
+    load_x(0).start()
     load_r.start()
     load_n.start()
     load_w.start()
     load_q.start()
     load_c.start()
+    for j in range(1, tpn):
+        load_x(j).start()
     load_g.start()
     load_u.start()
     load_d.start()
@@ -143,15 +149,27 @@
         return remote(kv.at[src], kv.at[src], kvs.at[half + s], kvr.at[half + s], mate, t)
 
     def source(s):
-        return lax.rem(e - s + n, n)
+        s = jnp.int32(s)
+        flipped = jnp.int32(0)
+        bit = 1
+        while bit < n:
+            ours = lax.rem(lax.div(e, jnp.int32(bit)), jnp.int32(2))
+            theirs = lax.rem(lax.div(s, jnp.int32(bit)), jnp.int32(2))
+            flipped = flipped + bit * (ours + theirs - 2 * ours * theirs)
+            bit *= 2
+        return flipped
 
     def send_a(s):
-        dst = lax.rem(e + s, n)
+        dst = source(s)
         return remote(sbuf.at[dst], recv.at[e, t], a_s.at[s], a_r.at[s], dst, t)
+
+    def send_near(s):
+        dst = source(s)
+        return remote(sbuf2.at[dst], recv.at[e, peer], bx_s.at[s], bx_r.at[s], dst, t)
 
     def copy_a(s):
         src = source(s)
-        return remote(sbuf.at[src], recv.at[src, t], a_s.at[s], a_r.at[s], lax.rem(e + s, n), t)
+        return remote(sbuf.at[src], recv.at[src, t], a_s.at[s], a_r.at[s], src, t)
 
     def copy_bx(s, col):
         src = source(s)
@@ -180,15 +198,10 @@
         return remote(s3.at[src], rbuf.at[e], r3_s.at[s], r3_r.at[s], src, t)
 
     def copy_r3_in(s):
-        src = lax.rem(e + s, n)
-        return remote(s3.at[src], rbuf.at[src], r3_s.at[s], r3_r.at[s], source(s), t)
-
-    load_k.wait()
-    load_v.wait()
+        src = source(s)
+        return remote(s3.at[src], rbuf.at[src], r3_s.at[s], r3_r.at[s], src, t)
+
     pl.semaphore_wait(barrier, n - 1 + tpn - 1)
-    for s in range(1, half):
-        kv_far(s).start()
-    kv_mate(0).start()
 
     lanes = 2 * n * cap
     place = lax.broadcasted_iota(jnp.int32, (own_rows, lanes), 1).astype(jnp.float32) + 0.5
@@ -197,28 +210,66 @@
     right = inside >= cap
     slot = jnp.where(right, inside - cap, inside)
     top, share = routes_ref.shape
-    own = lax.broadcasted_iota(jnp.int32, (own_rows, share), 1) == (
-        lax.broadcasted_iota(jnp.int32, (own_rows, share), 0) + t * own_rows
-    )
-
-    def column(line):
+
+    def column(line, j):
+        at = lax.rem(t + j, tpn) * own_rows
+        own = lax.broadcasted_iota(jnp.int32, (own_rows, share), 1) == (
+            lax.broadcasted_iota(jnp.int32, (own_rows, share), 0) + at
+        )
         return jnp.sum(
             jnp.where(own, jnp.broadcast_to(line, own.shape), 0.0), axis=1, keepdims=True
         )
 
-    load_r.wait()
-    named = [
-        column(routes_ref[k : k + 1, :].astype(jnp.float32)) == expert for k in range(top)
-    ]
-    total = sum([m.astype(jnp.float32) for m in named])
+    def route(k, j):
+        return column(routes_ref[k : k + 1, :].astype(jnp.float32), j)
+
     before = lax.broadcasted_iota(jnp.int32, (own_rows, own_rows), 1) < lax.broadcasted_iota(
         jnp.int32, (own_rows, own_rows), 0
     )
-    rank = jnp.dot(
-        before.astype(jnp.bfloat16), total.astype(jnp.bfloat16), preferred_element_type=jnp.float32
-    )
-    hit = rank == slot
-    chosen = jnp.where(hit, total, 0.0)
+
+    def choose(j):
+        named = [route(k, j) == expert for k in range(top)]
+        total = sum([m.astype(jnp.float32) for m in named])
+        rank = jnp.dot(
+            before.astype(jnp.bfloat16),
+            total.astype(jnp.bfloat16),
+            preferred_element_type=jnp.float32,
+        )
+        hit = rank == slot
+        chosen = jnp.where(hit, total, 0.0)
+        spread = jnp.concatenate(
+            [jnp.where(right, 0.0, chosen), jnp.where(right, chosen, 0.0)], axis=0
+        )
+        return spread.T.astype(jnp.bfloat16), hit, named
+
+    load_r.wait()
+    spread, hit, named = choose(0)
+    load_n.wait()
+    gain = gain_ref[...].astype(jnp.float32)
+    gain = jnp.concatenate([gain[j : j + 1, :] for j in range(gain.shape[0])], axis=1)
+
+    def halves(j):
+        load_x(j).wait()
+        x = xbuf[j].astype(jnp.float32)
+        scale = lax.rsqrt(jnp.mean(x * x, axis=-1, keepdims=True) + 1e-06)
+        normed = (x * scale * gain).astype(jnp.bfloat16)
+        return jnp.concatenate([normed[:, :wide], normed[:, wide:]], axis=0)
+
+    stacked = halves(0)
+    outgoing = jnp.dot(spread, stacked, preferred_element_type=jnp.float32)
+    sbuf[...] = outgoing.astype(jnp.bfloat16).reshape(sbuf.shape)
+    for s in range(half, n):
+        send_a(s).start()
+    for s in range(1, half):
+        send_a(s).start()
+    keep = pltpu.make_async_copy(sbuf.at[e], recv.at[e, t], lsem.at[7])
+    keep.start()
+    outgoing = jnp.dot(choose(2)[0], halves(2), preferred_element_type=jnp.float32)
+    sbuf2[...] = outgoing.astype(jnp.bfloat16).reshape(sbuf2.shape)
+    for s in range(1, half):
+        send_near(s).start()
+    recv[e, peer] = sbuf2[e]
+    keep.wait()
     for k in range(top):
         mine = jnp.where(hit & named[k], 1.0, 0.0)
         sel[2 * k * own_rows : (2 * k + 1) * own_rows, :] = jnp.where(right, 0.0, mine).astype(
@@ -227,73 +278,33 @@
         sel[(2 * k + 1) * own_rows : (2 * k + 2) * own_rows, :] = jnp.where(
             right, mine, 0.0
         ).astype(jnp.bfloat16)
-    spread = jnp.concatenate(
-        [jnp.where(right, 0.0, chosen), jnp.where(right, chosen, 0.0)], axis=0
-    )
-    spread = spread.T.astype(jnp.bfloat16)
-    load_x.wait()
-    load_n.wait()
-    x = xbuf[...].astype(jnp.float32)
-    gain = gain_ref[...].astype(jnp.float32)
-    gain = jnp.concatenate([gain[j : j + 1, :] for j in range(gain.shape[0])], axis=1)
-    scale = lax.rsqrt(jnp.mean(x * x, axis=-1, keepdims=True) + 1e-06)
-    normed = (x * scale * gain).astype(jnp.bfloat16)
-    stacked = jnp.concatenate([normed[:, :wide], normed[:, wide:]], axis=0)
-    outgoing = jnp.dot(spread, stacked, preferred_element_type=jnp.float32)
-    sbuf[...] = outgoing.astype(jnp.bfloat16).reshape(sbuf.shape)
-    for s in range(1, n):
-        send_a(s).start()
-    keep = pltpu.make_async_copy(sbuf.at[e], recv.at[e, t], lsem.at[7])
-    keep.start()
-    keep.wait()
-    copy_bx(0, t).start()
-    copy_bc(0, t).start()
-
+    load_k.wait()
+    load_v.wait()
     for s in range(1, half):
-        kv_far_in(s).wait_recv()
-        kv_mate(s).start()
-    for s in range(half):
-        kv_mate_in(s).wait_recv()
-    load_q.wait()
-    load_c.wait()
-    own_gate = gate_ref[:, pl.ds(pl.multiple_of(e * seq, seq), seq)]
-    eye = lax.broadcasted_iota(jnp.int32, (seq, seq), 0) == lax.broadcasted_iota(
-        jnp.int32, (seq, seq), 1
-    )
-    gate_col = jnp.sum(
-        jnp.where(eye, jnp.broadcast_to(own_gate, (seq, seq)), 0.0), axis=1, keepdims=True
-    )
-    key_pos = lax.broadcasted_iota(jnp.int32, (seq, n * seq), 1)
-    query_pos = lax.broadcasted_iota(jnp.int32, (seq, n * seq), 0) + e * seq
-    bias = gate_col - gate_ref[...]
-    group = q_ref.shape[1] // head
-    heads_out = []
-    for g in range(group):
-        q = q_ref[:, g * head : (g + 1) * head]
-        scores = jnp.concatenate(
-            [
-                jnp.dot(q, kv[j, 0:head, :], preferred_element_type=jnp.float32)
-                for j in range(n)
-            ],
-            axis=1,
-        )
-        scores = scores * (head ** (-0.5)) + bias
-        scores = jnp.where(key_pos <= query_pos, scores, -jnp.inf)
-        weights = jnp.exp(scores - jnp.max(scores, axis=-1, keepdims=True))
-        whole = jnp.sum(weights, axis=-1, keepdims=True)
-        weights = weights.astype(jnp.bfloat16)
-        summed = jnp.zeros((seq, head), jnp.float32)
-        for j in range(n):
-            summed = summed + lax.dot_general(
-                weights[:, j * seq : (j + 1) * seq],
-                kv[j, head : 2 * head, :],
-                (((1,), (1,)), ((), ())),
-                preferred_element_type=jnp.float32,
-            )
-        heads_out.append(summed / whole)
-    attended = jnp.concatenate(heads_out, axis=1).astype(jnp.bfloat16)
-    att[...] = attended.reshape(att.shape)
-    attr[t] = att[t]
+        kv_far(s).start()
+    kv_mate(0).start()
+
+    lane = lax.broadcasted_iota(jnp.int32, (own_rows, 2 * cap), 1)
+    lane_right = lane >= cap
+    lane_slot = jnp.where(lane_right, lane - cap, lane).astype(jnp.float32)
+    mine_expert = e.astype(jnp.float32)
+    for j in (1, 3):
+        hits = sum(
+            [jnp.where(route(k, j) == mine_expert, 1.0, 0.0) for k in range(top)]
+        )
+        hits = jnp.broadcast_to(hits, lane.shape)
+        ranks = jnp.dot(
+            before.astype(jnp.bfloat16),
+            hits.astype(jnp.bfloat16),
+            preferred_element_type=jnp.float32,
+        )
+        here = jnp.where(ranks == lane_slot, hits, 0.0)
+        here = jnp.concatenate(
+            [jnp.where(lane_right, 0.0, here), jnp.where(lane_right, here, 0.0)], axis=0
+        )
+        recv[e, lax.rem(t + j, tpn)] = jnp.dot(
+            here.T.astype(jnp.bfloat16), halves(j), preferred_element_type=jnp.float32
+        ).astype(jnp.bfloat16)
 
     def copy_att(s):
         dst = lax.rem(t + s, tpn)
@@ -303,30 +314,100 @@
         src = lax.rem(t - s + tpn, tpn)
         return remote(att.at[src], attr.at[src], ats.at[s], atr.at[s], e, lax.rem(t + s, tpn))
 
-    for s in range(1, tpn):
-        copy_att(s).start()
+    def attention():
+        for s in range(half):
+            kv_mate_in(s).wait_recv()
+        load_q.wait()
+        load_c.wait()
+        own_gate = gate_ref[:, pl.ds(pl.multiple_of(e * seq, seq), seq)]
+        eye = lax.broadcasted_iota(jnp.int32, (seq, seq), 0) == lax.broadcasted_iota(
+            jnp.int32, (seq, seq), 1
+        )
+        gate_col = jnp.sum(
+            jnp.where(eye, jnp.broadcast_to(own_gate, (seq, seq)), 0.0), axis=1, keepdims=True
+        )
+        key_pos = lax.broadcasted_iota(jnp.int32, (seq, n * seq), 1)
+        query_pos = lax.broadcasted_iota(jnp.int32, (seq, n * seq), 0) + e * seq
+        bias = gate_col - gate_ref[...]
+        group = q_ref.shape[1] // head
+        heads_out = []
+        for g in range(group):
+            q = q_ref[:, g * head : (g + 1) * head]
+            scores = jnp.concatenate(
+                [
+                    jnp.dot(q, kv[j, 0:head, :], preferred_element_type=jnp.float32)
+                    for j in range(n)
+                ],
+                axis=1,
+            )
+            scores = scores * (head ** (-0.5)) + bias
+            scores = jnp.where(key_pos <= query_pos, scores, -jnp.inf)
+            weights = jnp.exp(scores - jnp.max(scores, axis=-1, keepdims=True))
+            whole = jnp.sum(weights, axis=-1, keepdims=True)
+            weights = weights.astype(jnp.bfloat16)
+            summed = jnp.zeros((seq, head), jnp.float32)
+            for j in range(n):
+                summed = summed + lax.dot_general(
+                    weights[:, j * seq : (j + 1) * seq],
+                    kv[j, head : 2 * head, :],
+                    (((1,), (1,)), ((), ())),
+                    preferred_element_type=jnp.float32,
+                )
+            heads_out.append(summed / whole)
+        attended = jnp.concatenate(heads_out, axis=1).astype(jnp.bfloat16)
+        att[...] = attended.reshape(att.shape)
+        attr[t] = att[t]
+        for s in range(1, tpn):
+            copy_att(s).start()
+
     load_g.wait()
     load_u.wait()
     load_d.wait()
 
     def step(i, carry):
-        @pl.when((i >= 1) & (i < n))
+        @pl.when(i == n - 2)
         def _():
-            copy_a(i).wait_recv()
-            copy_bx(i, t).start()
-            copy_bc(i, t).start()
+            for s in range(1, half):
+                kv_far_in(s).wait_recv()
+                kv_mate(s).start()
+
+        @pl.when(i == n)
+        def _():
+            attention()
+
+        @pl.when(i < n)
+        def _():
+            s = lax.rem(i + half, n)
+
+            @pl.when(s > 0)
+            def _():
+                copy_a(s).wait_recv()
+
+                @pl.when(s >= half)
+                def _():
+                    copy_bx(s, t).start()
+
+                copy_bc(s, t).start()
 
         @pl.when((i >= 1) & (i <= n))
         def _():
-            copy_bx(i - 1, peer).wait_recv()
-            copy_c(i - 1, peer).start()
+            s = lax.rem(i - 1 + half, n)
+
+            @pl.when(s > 0)
+            def _():
+                copy_bx(s, peer).wait_recv()
+                copy_c(s, peer).start()
 
         @pl.when((i >= 2) & (i <= n + 1))
         def _():
-            s = i - 2
+            s = lax.rem(i - 2 + half, n)
             src = source(s)
-            copy_bc(s, partner).wait_recv()
-            copy_c(s, opp).wait_recv()
+
+            @pl.when(s > 0)
+            def _():
+                copy_bc(s, partner).wait_recv()
+                copy_c(s, opp).wait_recv()
+
             block = recv[src].astype(jnp.float32)
             count = block.shape[0] * cap
             lo = block[:, :cap].reshape(count, wide).astype(jnp.bfloat16)
@@ -348,7 +429,7 @@
 
         @pl.when((i >= 3) & (i <= n + 2))
         def _():
-            s = i - 3
+            s = lax.rem(i - 3 + half, n)
             src = source(s)
             copy_r1(s, 1, opp).wait_recv()
             copy_r1(s, 0, partner).wait_recv()
@@ -359,7 +440,7 @@
 
         @pl.when(i >= 4)
         def _():
-            s = i - 4
+            s = lax.rem(i - 4 + half, n)
             src = source(s)
             copy_r2(s).wait_recv()
             s3[src] = (
@@ -378,7 +459,7 @@
 
         return carry
 
-    lax.fori_loop(1, n + 4, step, 0)
+    lax.fori_loop(0, n + 4, step, 0)
 
     for s in range(1, tpn):
         copy_att_in(s).wait_recv()
@@ -394,7 +475,7 @@
         sel[...], rbuf[...].reshape(lanes, wide), preferred_element_type=jnp.float32
     )
     load_w.wait()
-    rw = [column(rw_ref[k : k + 1, :]) for k in range(top)]
+    rw = [column(rw_ref[k : k + 1, :], 0) for k in range(top)]
     for h in range(2):
         acc = jnp.zeros((own_rows, wide), jnp.float32)
         for k in range(top):
@@ -410,9 +491,6 @@
         copy_att(s).wait_send()
 
     def drain(s, carry):
-        copy_bx(s, t).wait_send()
-        copy_bc(s, t).wait_send()
-        copy_c(s, peer).wait_send()
         copy_r1(s, 0, partner).wait_send()
         copy_r1(s, 1, opp).wait_send()
         copy_r2(s).wait_send()
@@ -420,6 +498,9 @@
         @pl.when(s > 0)
         def _():
             send_a(s).wait_send()
+            copy_bx(s, t).wait_send()
+            copy_bc(s, t).wait_send()
+            copy_c(s, peer).wait_send()
             copy_r3(s).wait_send()
 
         return carry
@@ -470,7 +551,7 @@
             pltpu.VMEM((width // 128, 128), bf16),
             pltpu.VMEM((top, tpn * own_rows), jnp.int32),
             pltpu.VMEM((top, tpn * own_rows), jnp.float32),
-            pltpu.VMEM((own_rows, width), bf16),
+            pltpu.VMEM((tpn, own_rows, width), bf16),
             pltpu.VMEM((width, units), bf16),
             pltpu.VMEM((width, units), bf16),
             pltpu.VMEM((units, width), bf16),
@@ -480,6 +561,7 @@
             pltpu.VMEM((tpn, seq // tpn, queries.shape[1]), bf16),
             pltpu.VMEM((2 * top * own_rows, 2 * n * cap), bf16),
             pltpu.VMEM((n,) + chunk, bf16),
+            pltpu.VMEM((n,) + chunk, bf16),
             pltpu.VMEM((n, tpn) + chunk, bf16),
             pltpu.VMEM((n, tpn) + chunk, bf16),
             pltpu.VMEM((n, 2) + chunk, bf16),
@@ -487,7 +569,7 @@
             pltpu.VMEM((n,) + chunk, bf16),
             pltpu.VMEM((n,) + chunk, bf16),
             pltpu.VMEM((n,) + chunk, bf16),
-            dma((13,)),
+            dma((12 + tpn,)),
             dma((n,)),
             dma((n,)),
             dma((tpn,)),
@@ -690,7 +772,8 @@
     cap = block_capacity(own_rows, routes.shape[1], n * expert_gate.shape[0])
     fits = (
         tpn == 4
-        and n % 2 == 0
+        and n >= 4
+        and n & (n - 1) == 0
         and cap % 8 == 0
         and expert_gate.shape[0] == 1
         and key_cache.shape[0] == 1

time: 68.3 us -> 61.8 us (0.905)
  Pallas kernels: 64.2 us -> 57.8 us
    pallas_call x1, Pallas kernels: 64.2 us -> 57.8 us  [fused_body(): pl.pallas_call(functools.partial(fused_kernel, n, tpn, cap), out_shape=(j...]
where the time goes in v3:
time: 61.8 us; the launch traced here: 61.7 us
  Pallas kernels  57.8 us (94%)
  local copies, waits for them, and re-layouts  3.24 us (5%)
  between operations  0.64 us (1%)
    pallas_call x1, Pallas kernels, fused_body(): pl.pallas_call(functools.partial(fused_kernel, n, tpn, cap), out_shape=(j...  57.8 us
    unnamed x2, local copies, waits for them, and re-layouts  3.24 us

profile of v3, /device:TPU:0, one launch (start us, length us, event | category | flops | bytes accessed | tf_op | source)
XLA Modules:
  0.0 61.7 jit_solution(8090113178758762656)
XLA Ops:
  0.6 57.8 %shard_map.131 = (bf16[32,2048]{1,0:T(8,128)(2,1)}, bf16[64,2048]{1,0:T(8,128)(2,1)}) custom-call(bf16[128,128]{1,0:T(8,128)(2,1)} %q_any.1, f32[1,1024]{1,0:T(1,128)} %gate_any.1, bf16[16,128]{1,0:T(8,128)(2,1)} %bitcast.3, s32[2,256]{1,0:T(2,128)} %bitcast.4, f32[2,256]{1,0:T(2,128)} %bitcast.5, bf16[1,64,128]{2,1,0:T(8,128)(2,1)} %k_any.1, ...), custom_call_target="tpu_custom_call" | custom-call | tf_op jit(solution)/shard_map/pallas_call | solution.py:540
  58.4 1.6 %copy.16 = bf16[32,2048]{1,0:T(8,128)(2,1)} copy(bf16[32,2048]{1,0:T(8,128)(2,1)} %get-tuple-element.4) | data formatting | bytes 262144
  60.0 1.7 %copy.17 = bf16[64,2048]{1,0:T(8,128)(2,1)} copy(bf16[64,2048]{1,0:T(8,128)(2,1)} %get-tuple-element.5) | data formatting | bytes 524288

commit v4 on v3

--- a/solution.py
+++ b/solution.py
@@ -364,6 +364,11 @@
     load_u.wait()
     load_d.wait()
 
+    def order(p):
+        skip = lax.div(p, jnp.int32(half + 1))
+        later = lax.div(p + n - 1, jnp.int32(n))
+        return later * lax.rem(p + half - 1 + skip, n)
+
     def step(i, carry):
         @pl.when(i == n - 2)
         def _():
@@ -377,7 +382,7 @@
 
         @pl.when(i < n)
         def _():
-            s = lax.rem(i + half, n)
+            s = order(i)
 
             @pl.when(s > 0)
             def _():
@@ -391,7 +396,7 @@
 
         @pl.when((i >= 1) & (i <= n))
         def _():
-            s = lax.rem(i - 1 + half, n)
+            s = order(i - 1)
 
             @pl.when(s > 0)
             def _():
@@ -400,7 +405,7 @@
 
         @pl.when((i >= 2) & (i <= n + 1))
         def _():
-            s = lax.rem(i - 2 + half, n)
+            s = order(i - 2)
             src = source(s)
 
             @pl.when(s > 0)
@@ -429,7 +434,7 @@
 
         @pl.when((i >= 3) & (i <= n + 2))
         def _():
-            s = lax.rem(i - 3 + half, n)
+            s = order(i - 3)
             src = source(s)
             copy_r1(s, 1, opp).wait_recv()
             copy_r1(s, 0, partner).wait_recv()
@@ -440,7 +445,7 @@
 
         @pl.when(i >= 4)
         def _():
-            s = lax.rem(i - 4 + half, n)
+            s = order(i - 4)
             src = source(s)
             copy_r2(s).wait_recv()
             s3[src] = (

time: 61.8 us -> 59.8 us (0.968)
  Pallas kernels: 57.8 us -> 55.8 us
    pallas_call x1, Pallas kernels: 57.8 us -> 55.8 us  [fused_body(): pl.pallas_call(functools.partial(fused_kernel, n, tpn, cap), out_shape=(j...]
where the time goes in v4:
time: 59.8 us; the launch traced here: 59.7 us
  Pallas kernels  55.8 us (93%)
  local copies, waits for them, and re-layouts  3.24 us (5%)
  between operations  0.64 us (1%)
    pallas_call x1, Pallas kernels, fused_body(): pl.pallas_call(functools.partial(fused_kernel, n, tpn, cap), out_shape=(j...  55.8 us
    unnamed x2, local copies, waits for them, and re-layouts  3.24 us

profile of v4, /device:TPU:0, one launch (start us, length us, event | category | flops | bytes accessed | tf_op | source)
XLA Modules:
  0.0 59.7 jit_solution(5988424667385391330)
XLA Ops:
  0.6 55.8 %shard_map.131 = (bf16[32,2048]{1,0:T(8,128)(2,1)}, bf16[64,2048]{1,0:T(8,128)(2,1)}) custom-call(bf16[128,128]{1,0:T(8,128)(2,1)} %q_any.1, f32[1,1024]{1,0:T(1,128)} %gate_any.1, bf16[16,128]{1,0:T(8,128)(2,1)} %bitcast.3, s32[2,256]{1,0:T(2,128)} %bitcast.4, f32[2,256]{1,0:T(2,128)} %bitcast.5, bf16[1,64,128]{2,1,0:T(8,128)(2,1)} %k_any.1, ...), custom_call_target="tpu_custom_call" | custom-call | tf_op jit(solution)/shard_map/pallas_call | solution.py:545
  56.4 1.6 %copy.16 = bf16[32,2048]{1,0:T(8,128)(2,1)} copy(bf16[32,2048]{1,0:T(8,128)(2,1)} %get-tuple-element.4) | data formatting | bytes 262144
  58.0 1.7 %copy.17 = bf16[64,2048]{1,0:T(8,128)(2,1)} copy(bf16[64,2048]{1,0:T(8,128)(2,1)} %get-tuple-element.5) | data formatting | bytes 524288
